TPU v7x, 32 devices: a whole 2x2x4 slice. The times are simulated.
32 devices in a mesh: dp: 4 (over y, x), kv: 4 (over z), tp: 2 (over core).
Axes of the slice: x: 2, y: 2, z: 4, core: 2. Of those that a mesh axis runs over, the one named last changes fastest.
Arguments:
- tokens: bfloat16 [96, 2048], P('dp', 'kv'), may hold values from -6 to 6
- norm_gain: float32 [2048], P('kv'), may hold values from 0.1 to 1.9
- w_query: bfloat16 [2048, 1024], P('kv', 'tp'), may hold values from -0.125 to 0.125
- w_key: bfloat16 [2048, 256], P('kv', 'tp'), may hold values from -0.125 to 0.125
- w_value: bfloat16 [2048, 256], P('kv', 'tp'), may hold values from -0.125 to 0.125
- head_bias: float32 [8], P('tp'), may hold values from -1.5 to 1
- cache_key: bfloat16 [96, 2048, 2, 128], P('dp', 'kv', 'tp'), may hold values from -6 to 6
- cache_value: bfloat16 [96, 2048, 2, 128], P('dp', 'kv', 'tp'), may hold values from -6 to 6
- lengths: int32 [96], P('dp'), may hold values from 1 to 2047
- w_out: bfloat16 [1024, 2048], P('tp', 'kv'), may hold values from -0.1875 to 0.1875
Outputs:
- mixed: float32 [96, 2048], P('dp', 'kv')
- new_key: bfloat16 [96, 2, 128], P('dp', 'tp')
- new_value: bfloat16 [96, 2, 128], P('dp', 'tp')
Inputs may be any that keep to these rules, and one draw needn't show every extreme that they name: `lengths`: each length lies between 1 and 2047, so that the new token has a place in the cache.
All inputs are finite; a program needn't handle non-finite values.
Results may differ from a plain program's by a relative error of at most 0.001.
Values sent between devices are 32-bit elements.
A program may use at most 64 MiB of HBM per device.

v0:
```python
import math

import jax
import jax.numpy as jnp
from jax import lax
from jax.sharding import PartitionSpec as P

norm_eps = 1e-06
out_eps = 1e-08


def body(
    tokens, norm_gain, w_query, w_key, w_value, head_bias, cache_key, cache_value, lengths, w_out
):
    seq_count = tokens.shape[0]
    full_width = tokens.shape[1] * lax.axis_size("kv")
    floats_in = tokens.astype(jnp.float32)
    local_squares = jnp.sum(floats_in * floats_in, axis=1)
    scaled = (floats_in * norm_gain).astype(jnp.bfloat16)
    part_query = jnp.dot(scaled, w_query, preferred_element_type=jnp.float32)
    part_key = jnp.dot(scaled, w_key, preferred_element_type=jnp.float32)
    part_value = jnp.dot(scaled, w_value, preferred_element_type=jnp.float32)
    total_squares = lax.psum(local_squares, "kv")
    sum_query, sum_key, sum_value = lax.psum((part_query, part_key, part_value), "kv")
    inv_rms = lax.rsqrt(total_squares / full_width + norm_eps)[:, None]
    queries = (inv_rms * sum_query).astype(jnp.bfloat16)
    new_key = (inv_rms * sum_key).astype(jnp.bfloat16)
    new_value = (inv_rms * sum_value).astype(jnp.bfloat16)
    pos_local = cache_key.shape[1]
    kv_local = cache_key.shape[2]
    head_dim = cache_key.shape[3]
    heads_local = head_bias.shape[0]
    group_size = heads_local // kv_local
    all_positions = pos_local * lax.axis_size("kv")
    grouped = queries.reshape(seq_count, kv_local, group_size, head_dim)
    offsets = (head_bias - math.log(all_positions)).reshape(1, kv_local, group_size, 1)
    scores = (
        jnp.einsum("scgd,spcd->scgp", grouped, cache_key, preferred_element_type=jnp.float32)
        * head_dim ** (-0.5)
        + offsets
    )
    first_pos = lax.axis_index("kv") * pos_local
    positions = first_pos + jnp.arange(pos_local, dtype=jnp.int32)
    visible = (positions[None, :] < lengths[:, None])[:, None, None, :]
    penalty = jnp.where(visible, jax.nn.softplus(scores), 0.0)
    between = lax.cumsum(penalty, axis=3, reverse=True) - penalty
    weights = jnp.where(visible, jnp.exp(jax.nn.log_sigmoid(scores) - between), 0.0)
    weighted = jnp.einsum(
        "scgp,spcd->scgd", weights, cache_value.astype(jnp.float32), precision=lax.Precision.HIGHEST
    ).reshape(seq_count, heads_local, head_dim)
    decay_total = jnp.sum(penalty, axis=3).reshape(seq_count, heads_local)
    all_weighted, all_decay = (
        lax.all_gather(weighted[None], "kv", axis=0, tiled=True),
        lax.all_gather(decay_total[None], "kv", axis=0, tiled=True),
    )
    suffix = jnp.cumsum(all_decay[::-1], axis=0)[::-1] - all_decay
    attended = jnp.sum(all_weighted * jnp.exp(-suffix)[:, :, :, None], axis=0)
    attended = attended.reshape(seq_count, heads_local * head_dim)
    partial_out = jnp.dot(
        attended,
        w_out.astype(jnp.float32),
        preferred_element_type=jnp.float32,
        precision=lax.Precision.HIGHEST,
    )
    projected = lax.psum(partial_out, "tp")
    out_squares = lax.psum(jnp.sum(projected * projected, axis=1), "kv")
    mixed = projected * lax.rsqrt(out_squares / full_width + out_eps)[:, None]
    return (
        mixed,
        new_key.reshape(seq_count, kv_local, head_dim),
        new_value.reshape(seq_count, kv_local, head_dim),
    )


def solution(mesh):
    placed = (
        P("dp", "kv"),
        P("kv"),
        P("kv", "tp"),
        P("kv", "tp"),
        P("kv", "tp"),
        P("tp"),
        P("dp", "kv", "tp", None),
        P("dp", "kv", "tp", None),
        P("dp"),
        P("tp", "kv"),
    )
    return jax.shard_map(
        body,
        mesh=mesh,
        in_specs=placed,
        out_specs=(P("dp", "kv"), P("dp", "tp", None), P("dp", "tp", None)),
        check_vma=False,
    )
```

profile of v0, /device:TPU:0, one launch (start us, length us, event | category | flops | bytes accessed | tf_op | source)
XLA Modules:
  0.0 121.7 jit_solution(6466097838132708483)
XLA Ops:
  0.6 0.0 copy-start
  0.6 0.0 copy-start.3
  0.7 1.4 %fusion.35 = f32[24,512]{1,0:T(8,128)S(1)} fusion(bf16[512,512]{1,0:T(8,128)(2,1)} %param.12, bf16[24,512]{1,0:T(8,128)(2,1)} %param.10, f32[512]{0:T(512)} %param.11), kind=kOutput, calls=%fused_computation.39 | convolution fusion | flops 12619776 | bytes 600064 | tf_op jit(solution)/shard_map/dot_general | solution.py:20
  2.1 0.9 fusion.26
  2.9 21.6 %all-reduce.1 = (f32[24,512]{1,0:T(8,128)S(1)}, f32[24]{0:T(128)S(1)}) all-reduce(f32[24,512]{1,0:T(8,128)S(1)} %fusion.35, f32[24]{0:T(128)S(1)} %fusion.26), channel_id=1, replica_groups=mesh['dp'=4,'kv'=4,'tp'=2] {'kv'}, use_global_device_ids=true, to_apply=%region_2.0 | all-reduce | flops 12312 | bytes 98496 | tf_op jit(solution)/shard_map/psum | solution.py:24
  24.5 0.0 copy-start.2
  24.5 0.1 multiply_convert_fusion
  24.6 0.5 copy-done.2
  25.1 0.7 broadcast_add_fusion
  25.7 0.0 copy-done
  25.7 1.5 %convert_reduce_fusion = (u32[4,512]{1,0:T(4,128)}, f32[24,4,512]{2,1,0:T(4,128)S(1)}) fusion(f32[4]{0:T(128)S(1)} %broadcast_add_fusion, bf16[24,4,128]{2,1,0:T(4,128)(2,1)S(1)} %reshape.115, bf16[24,512,1,128]{3,1,2,0:T(8,128)(2,1)S(1)} %copy-done), kind=kOutput, calls=%fused_computation.12 | convolution fusion | flops 12875776 | bytes 3375120 | tf_op jit(solution)/shard_map/scgd,spcd->scgp/dot_general | solution.py:38
  27.3 0.0 copy-done.3
  27.3 0.1 broadcast_compare_fusion
  27.3 1.7 %fusion.40 = (f32[24,4]{1,0:T(8,128)}, f32[24,4,512]{2,1,0:T(4,128)S(1)}) fusion(f32[24,4,512]{2,1,0:T(4,128)S(1)} %get-tuple-element.13, u32[4,512]{1,0:T(4,128)} %get-tuple-element.12, pred[24,512]{1,0:T(8,128)(4,1)S(1)} %broadcast_compare_fusion), kind=kLoop, calls=%fused_computation.51 | loop fusion | flops 491424 | bytes 414080 | tf_op jit(solution)/shard_map/reduce_sum | solution.py:51
  29.0 0.8 reshape.117
  29.8 1.7 %copy.22 = f32[24,1,4,4,128]{4,0,2,1,3:T(8,128)} copy(f32[24,1,4,4,128]{4,3,2,0,1:T(4,128)} %reshape.117) | data formatting | bytes 393216 | tf_op jit(solution)/shard_map/reshape
  31.5 21.2 %reduce-window.6 = f32[24,1,4,4,128]{4,0,2,1,3:T(8,128)} reduce-window(f32[24,1,4,4,128]{4,0,2,1,3:T(8,128)} %copy.22, f32[]{:T(128)} %constant.26.clone.1), window={size=1x1x1x1x128 pad=0_0x0_0x0_0x0_0x0_127}, to_apply=%region_3.0 | reduce-window | flops 6242304 | bytes 393220 | tf_op jit(solution)/shard_map/reduce-window
  52.7 1.7 %copy.24 = f32[24,1,4,4,1]{0,3,4,2,1:T(4,128)} copy(f32[24,1,4,4,1]{4,0,2,1,3:T(8,128)} %bitcast.34) | data formatting | bytes 3072 | tf_op jit(solution)/shard_map/slice
  54.3 1.3 %reduce-window.9 = f32[24,1,4,5]{0,3,2,1:T(8,128)} reduce-window(f32[24,1,4,4]{0,3,2,1:T(4,128)} %bitcast.37, f32[]{:T(128)} %constant.26.clone.1), window={size=1x1x1x4 pad=0_0x0_0x0_0x0_4}, to_apply=%region_4.0 | reduce-window | flops 1440 | bytes 3460 | tf_op jit(solution)/shard_map/reduce-window.1
  55.7 1.3 %slice_bitcast_fusion = f32[24,4,4]{0,2,1:T(4,128)} fusion(f32[24,1,4,5]{0,3,2,1:T(8,128)} %reduce-window.9), kind=kLoop, calls=%fused_computation.42 | loop fusion | bytes 3072 | tf_op jit(solution)/shard_map/reshape.17
  57.0 1.4 %copy.25 = f32[24,4,4]{2,1,0:T(4,128)} copy(f32[24,4,4]{0,2,1:T(4,128)} %slice_bitcast_fusion) | data formatting | bytes 3072 | tf_op jit(solution)/shard_map/reshape.17
  58.4 1.6 %broadcast.59 = f32[24,4,4,128]{3,2,1,0:T(4,128)} broadcast(f32[24,4,4]{2,1,0:T(4,128)} %copy.25), dimensions={0,1,2} | broadcast | bytes 198144 | tf_op jit(solution)/shard_map/broadcast.24
  60.0 1.7 %reshape.121 = f32[24,4,512]{2,1,0:T(4,128)} reshape(f32[24,4,4,128]{3,2,1,0:T(4,128)} %broadcast.59) | data formatting | bytes 393216 | tf_op jit(solution)/shard_map/reshape.56
  61.7 0.0 copy-start.1
  61.7 1.7 %copy.23 = f32[24,1,4,4,128]{4,3,2,0,1:T(4,128)} copy(f32[24,1,4,4,128]{4,0,2,1,3:T(8,128)} %reduce-window.6) | data formatting | bytes 393216 | tf_op jit(solution)/shard_map/reduce-window
  63.5 1.7 %reshape.118 = f32[24,4,512]{2,1,0:T(4,128)} reshape(f32[24,1,4,4,128]{4,3,2,0,1:T(4,128)} %copy.23) | data formatting | bytes 393216 | tf_op jit(solution)/shard_map/reshape.55
  65.2 3.6 %fusion = f32[24,4,128]{2,1,0:T(4,128)S(1)} fusion(bf16[24,512,1,128]{3,1,2,0:T(8,128)(2,1)} %param.17, f32[24,4,512]{2,1,0:T(4,128)S(1)} %get-tuple-element.9, f32[24,4,512]{2,1,0:T(4,128)} %reshape.118, f32[24,4,512]{2,1,0:T(4,128)} %reshape.121, f32[24,4,512]{2,1,0:T(4,128)S(1)} %get-tuple-element.13, pred[24,512]{1,0:T(8,128)(4,1)S(1)} %broadcast_compare_fusion), kind=kOutput, calls=%fused_computation | convolution fusion | flops 76087296 | bytes 3993600 | tf_op jit(solution)/shard_map/scgp,spcd->scgd/dot_general | solution.py:48
  68.8 13.8 %all-gather = f32[96,4,128]{2,1,0:T(4,128)S(1)} all-gather(f32[24,4,128]{2,1,0:T(4,128)S(1)} %fusion), channel_id=2, replica_groups=mesh['dp'=4,'kv'=4,'tp'=2] {'kv'}, dimensions={0}, use_global_device_ids=true | all-gather | bytes 245760 | tf_op jit(solution)/shard_map/all_gather | solution.py:53
  82.6 0.8 copy.26
  83.4 13.0 %all-gather.2 = f32[4,24,4]{1,2,0:T(4,128)S(1)} all-gather(f32[1,24,4]{1,2,0:T(4,128)S(1)} %bitcast.38), channel_id=3, replica_groups=mesh['dp'=4,'kv'=4,'tp'=2] {'kv'}, dimensions={0}, use_global_device_ids=true | all-gather | bytes 1920 | tf_op jit(solution)/shard_map/all_gather | solution.py:54
  96.5 0.1 copy.27
  96.6 0.2 multiply_reduce_fusion
  96.8 1.4 %fusion.28 = f32[24,512]{1,0:T(8,128)S(1)} fusion(bf16[512,512]{1,0:T(8,128)(2,1)} %param.19, f32[3,8,4,128]{3,2,1,0:T(4,128)S(1)} %bitcast.36), kind=kOutput, calls=%fused_computation.30 | convolution fusion | flops 75497472 | bytes 622592 | tf_op jit(solution)/shard_map/dot_general | solution.py:59
  98.1 3.5 %psum.44 = f32[24,512]{1,0:T(8,128)S(1)} all-reduce(f32[24,512]{1,0:T(8,128)S(1)} %fusion.28), channel_id=1, replica_groups=mesh['dp'=4,'kv'=4,'tp'=2] {'tp'}, use_global_device_ids=true, to_apply=%region_8.9 | all-reduce | flops 12288 | bytes 98304 | tf_op jit(solution)/shard_map/psum | solution.py:65
  101.7 0.1 multiply_reduce_fusion.1
  101.8 0.0 copy-done.1
  101.8 1.1 fusion.31
  102.9 1.1 fusion.33
  103.9 15.8 %all-reduce = (f32[24]{0:T(128)S(1)}, f32[24,128]{1,0:T(8,128)S(1)}, f32[24,128]{1,0:T(8,128)S(1)}) all-reduce(f32[24]{0:T(128)S(1)} %multiply_reduce_fusion.1, f32[24,128]{1,0:T(8,128)S(1)} %fusion.33, f32[24,128]{1,0:T(8,128)S(1)} %fusion.31), channel_id=1, replica_groups=mesh['dp'=4,'kv'=4,'tp'=2] {'kv'}, use_global_device_ids=true, to_apply=%region_10.11 | all-reduce | flops 6168 | bytes 49344 | tf_op jit(solution)/shard_map/psum | solution.py:66
  119.7 1.3 %fusion.38 = (bf16[24,1,128]{2,0,1:T(8,128)(2,1)}, bf16[24,1,128]{2,0,1:T(8,128)(2,1)}) fusion(f32[24,128]{1,0:T(8,128)S(1)} %get-tuple-element.5, f32[24]{0:T(128)} %copy-done.2, f32[24,128]{1,0:T(8,128)S(1)} %get-tuple-element.4), kind=kLoop, calls=%fused_computation.45 | loop fusion | flops 12288 | bytes 36960 | tf_op jit(solution)/shard_map/reshape | solution.py:71
  121.0 0.7 broadcast_multiply_fusion
  (7 shorter events, 0.1 us)
Async XLA Ops:
  0.6 25.1 %copy-start = (bf16[24,512,1,128]{3,1,2,0:T(8,128)(2,1)S(1)}, bf16[24,512,1,128]{3,1,2,0:T(8,128)(2,1)}, u32[]{:S(2)}) copy-start(bf16[24,512,1,128]{3,1,2,0:T(8,128)(2,1)} %param.16) | copy-start | bytes 9437188
  0.6 26.6 %copy-start.3 = (s32[24]{0:T(128)S(1)}, s32[24]{0:T(128)}, u32[]{:S(2)}) copy-start(s32[24]{0:T(128)} %param.18) | copy-start | bytes 292
  24.5 0.6 copy-start.2
  61.7 40.1 %copy-start.1 = (f32[512]{0:T(512)S(1)}, f32[512]{0:T(512)}, u32[]{:S(2)}) copy-start(f32[512]{0:T(512)} %param.11) | copy-start | bytes 6148
where the time goes:
time: 123 us; the launch traced here: 122 us
  blocking collectives  67.7 us (55%)
  other arithmetic  28.2 us (23%)
  local copies, waits for them, and re-layouts  15 us (12%)
  matrix products  10.1 us (8%)
    another operation x2, other arithmetic  22.5 us
    psum x1, blocking collectives, body(): lax.psum((part_query, part_key, part_value), 'kv')  21.6 us
    psum x1, blocking collectives, body(): out_squares = lax.psum(jnp.sum(projected * projected, axis=1), 'kv')  15.8 us
    all_gather x1, blocking collectives, body(): lax.all_gather(weighted[None], 'kv', axis=0, tiled=True)  13.8 us
    all_gather x1, blocking collectives, body(): lax.all_gather(decay_total[None], 'kv', axis=0, tiled=True)  13 us
    another operation x7, local copies, waits for them, and re-layouts  9.53 us
    dot_general x1, matrix products, body(): jnp.einsum('scgp,spcd->scgd', weights, cache_value.astype(jnp.float32), p...  3.65 us
    psum x1, blocking collectives, body(): projected = lax.psum(partial_out, 'tp')  3.53 us

commit v1 on v0

v1 whole, which is shorter than its diff:
```python
import functools
import math

import jax
import jax.numpy as jnp
from jax import lax
from jax.experimental import pallas as pl
from jax.experimental.pallas import tpu as pltpu
from jax.sharding import PartitionSpec as P

norm_eps = 1e-06
out_eps = 1e-08
f32 = jnp.float32
bf16 = jnp.bfloat16
SUB = 8
LANES = 128


def kernel(
    dims,
    tok_hbm, gain_hbm, wq_hbm, wk_hbm, wv_hbm, bias_ref, ck_hbm, cv_hbm, len_ref, wo_hbm,
    mixed_ref, nk_ref, nv_ref,
    tok, gain, wq, wkv, ck, cv, wo,
    got_q, got_kv, got_att, got_tp, got_sq, qs, pen_s, ls_s, out_s, tot_s,
    load_sem, key_sem, val_sem,
    send_q, recv_q, send_kv, recv_kv, send_att, recv_att, send_tp, recv_tp, send_sq, recv_sq,
):
    n_kv, n_tp, seqs, heads, head_dim, pos_local, chunks = dims
    me = lax.axis_index("kv")
    me_tp = lax.axis_index("tp")
    groups = seqs // SUB
    width_local = tok.shape[1]
    full_width = width_local * n_kv
    all_pos = pos_local * n_kv

    loads = [
        pltpu.make_async_copy(tok_hbm, tok, load_sem.at[0]),
        pltpu.make_async_copy(gain_hbm, gain, load_sem.at[1]),
        pltpu.make_async_copy(wq_hbm, wq, load_sem.at[2]),
        pltpu.make_async_copy(wk_hbm, wkv.at[0], load_sem.at[3]),
        pltpu.make_async_copy(wv_hbm, wkv.at[1], load_sem.at[4]),
    ]
    for c in loads:
        c.start()
    per = seqs // chunks
    keys = [pltpu.make_async_copy(ck_hbm.at[pl.ds(i * per, per)], ck.at[pl.ds(i * per, per)], key_sem.at[i]) for i in range(chunks)]
    vals = [pltpu.make_async_copy(cv_hbm.at[pl.ds(i * per, per)], cv.at[pl.ds(i * per, per)], val_sem.at[i]) for i in range(chunks)]
    load_wo = pltpu.make_async_copy(wo_hbm, wo, load_sem.at[5])
    for c in keys + vals:
        c.start()
    load_wo.start()

    barrier = pltpu.get_barrier_semaphore()
    for d in range(1, n_kv):
        pl.semaphore_signal(barrier, inc=1, device_id={"kv": lax.rem(me + d, n_kv)}, device_id_type=pl.DeviceIdType.MESH)
    for d in range(1, n_tp):
        pl.semaphore_signal(barrier, inc=1, device_id={"tp": lax.rem(me_tp + d, n_tp)}, device_id_type=pl.DeviceIdType.MESH)

    def spread(buf, send, recv, axis, me_axis, n):
        copies = []
        for d in range(1, n):
            copies.append(pltpu.make_async_remote_copy(
                src_ref=buf.at[0], dst_ref=buf.at[d], send_sem=send.at[d - 1], recv_sem=recv.at[d - 1],
                device_id={axis: lax.rem(me_axis + d, n)}, device_id_type=pl.DeviceIdType.MESH))
        return copies

    def slot_of(source):
        return lax.rem(me - source + n_kv, n_kv)

    lane = lax.broadcasted_iota(jnp.int32, (SUB, LANES), 1)

    def pack(columns):
        tile = jnp.zeros((SUB, LANES), f32)
        for c, column in enumerate(columns):
            tile = jnp.where(lane == c, column, tile)
        return tile

    def unpack(tile, count):
        return [jnp.sum(jnp.where(lane == c, tile, 0.0), axis=1, keepdims=True) for c in range(count)]

    loads[0].wait()
    loads[1].wait()
    x = tok[...].astype(f32)
    squares = jnp.sum(x * x, axis=1, keepdims=True)
    scaled = (x * gain[...]).astype(bf16)
    loads[2].wait()
    part_q = jnp.dot(scaled, wq[...], preferred_element_type=f32)
    for h in range(heads):
        got_q[0, h * seqs:(h + 1) * seqs, :] = part_q[:, h * head_dim:(h + 1) * head_dim]
    got_q[0, heads * seqs:, :] = pack([squares[c * SUB:(c + 1) * SUB] for c in range(groups)])
    pl.semaphore_wait(barrier, n_kv - 1 + n_tp - 1)
    copies_q = spread(got_q, send_q, recv_q, "kv", me, n_kv)
    for c in copies_q:
        c.start()
    loads[3].wait()
    loads[4].wait()
    for i in range(2):
        got_kv[0, i * seqs:(i + 1) * seqs, :] = jnp.dot(scaled, wkv[i], preferred_element_type=f32)
    copies_kv = spread(got_kv, send_kv, recv_kv, "kv", me, n_kv)
    for c in copies_kv:
        c.start()

    later = lax.broadcasted_iota(jnp.int32, (pos_local, pos_local), 0) > lax.broadcasted_iota(jnp.int32, (pos_local, pos_local), 1)
    tri = jnp.where(later, 1.0, 0.0).astype(bf16)
    row = lax.broadcasted_iota(jnp.int32, (2 * heads, 1), 0)
    offset = jnp.zeros((2 * heads, 1), f32)
    for h in range(heads):
        offset = jnp.where(lax.rem(row, heads) == h, bias_ref[h], offset)
    offset = offset - math.log(all_pos)
    high = lax.broadcasted_iota(jnp.int32, (2 * heads, pos_local), 0) < heads
    positions = me * pos_local + lax.broadcasted_iota(jnp.int32, (2 * heads, pos_local), 1)

    for c in copies_q:
        c.wait_recv()
    sum_q = got_q[slot_of(0)]
    for k in range(1, n_kv):
        sum_q = sum_q + got_q[slot_of(k)]
    inv = [lax.rsqrt(t / full_width + norm_eps) for t in unpack(sum_q[heads * seqs:, :], groups)]
    inv = jnp.concatenate(inv, axis=0)
    stride = 2 * heads
    for h in range(heads):
        q = (sum_q[h * seqs:(h + 1) * seqs, :] * inv).astype(bf16).astype(f32)
        qs[pl.ds(h, seqs, stride=stride), :] = q
        qs[pl.ds(heads + h, seqs, stride=stride), :] = q

    for s in range(seqs):
        if s % per == 0:
            keys[s // per].wait()
        rows = slice(s * stride, (s + 1) * stride)
        score = lax.dot_general(qs[rows, :].astype(bf16), ck[s], (((1,), (1,)), ((), ())), preferred_element_type=f32)
        score = score * head_dim ** (-0.5) + offset
        tail = jnp.log1p(jnp.exp(-jnp.abs(score)))
        visible = positions < len_ref[s]
        penalty = jnp.where(visible, jnp.maximum(score, 0.0) + tail, 0.0)
        top = penalty.astype(bf16).astype(f32)
        pen_s[rows, :] = jnp.where(high, top, penalty - top)
        ls_s[rows, :] = jnp.where(visible, jnp.minimum(score, 0.0) - tail, -1e30)
    suffix = jnp.dot(pen_s[...].astype(bf16), tri, preferred_element_type=f32)
    for s in range(seqs):
        if s % per == 0:
            vals[s // per].wait()
        rows = slice(s * stride, (s + 1) * stride)
        between = suffix[rows, :]
        between = between + pltpu.roll(between, heads, 0)
        weights = jnp.exp(ls_s[rows, :] - between)
        top = weights.astype(bf16).astype(f32)
        parts = jnp.where(high, top, weights - top).astype(bf16)
        out = jnp.dot(parts, cv[s], preferred_element_type=f32)
        out_s[rows, :] = out + pltpu.roll(out, heads, 0)
        first = pen_s[rows, 0:LANES]
        total = between[:, 0:LANES] + first + pltpu.roll(first, heads, 0)
        tot_s[rows, :] = total
    columns = []
    for h in range(heads):
        got_att[0, h * seqs:(h + 1) * seqs, :] = out_s[pl.ds(h, seqs, stride=stride), :]
        totals = tot_s[pl.ds(h, seqs, stride=stride), :]
        columns += [totals[c * SUB:(c + 1) * SUB, 0:1] for c in range(groups)]
    got_att[0, heads * seqs:, :] = pack(columns)
    copies_att = spread(got_att, send_att, recv_att, "kv", me, n_kv)
    for c in copies_att:
        c.start()

    for c in copies_kv:
        c.wait_recv()
    sum_kv = got_kv[slot_of(0)]
    for k in range(1, n_kv):
        sum_kv = sum_kv + got_kv[slot_of(k)]
    nk_ref[...] = (sum_kv[:seqs, :] * inv).astype(bf16)
    nv_ref[...] = (sum_kv[seqs:, :] * inv).astype(bf16)
    load_wo.wait()

    for c in copies_att:
        c.wait_recv()
    pieces = [None] * heads
    behind = jnp.zeros((SUB, LANES), f32)
    for k in reversed(range(n_kv)):
        slot = slot_of(k)
        factor = jnp.exp(-behind)
        behind = behind + got_att[slot, heads * seqs:, :]
        for h in range(heads):
            f = jnp.concatenate([factor[:, h * groups + c:h * groups + c + 1] for c in range(groups)], axis=0)
            term = got_att[slot, h * seqs:(h + 1) * seqs, :] * f
            pieces[h] = term if pieces[h] is None else pieces[h] + term
    attended = jnp.concatenate(pieces, axis=1)
    top = attended.astype(bf16).astype(f32)
    both = jnp.concatenate([top, attended - top], axis=0).astype(bf16)
    partial = jnp.dot(both, wo[...], preferred_element_type=f32)
    got_tp[0] = partial[:seqs, :] + partial[seqs:, :]
    copies_tp = spread(got_tp, send_tp, recv_tp, "tp", me_tp, n_tp)
    for c in copies_tp:
        c.start()
    for c in copies_tp:
        c.wait_recv()
    projected = got_tp[lax.rem(me_tp + n_tp, n_tp)]
    for k in range(1, n_tp):
        projected = projected + got_tp[lax.rem(me_tp - k + n_tp, n_tp)]
    squares = jnp.sum(projected * projected, axis=1, keepdims=True)
    got_sq[0] = pack([squares[c * SUB:(c + 1) * SUB] for c in range(groups)])
    copies_sq = spread(got_sq, send_sq, recv_sq, "kv", me, n_kv)
    for c in copies_sq:
        c.start()
    for c in copies_sq:
        c.wait_recv()
    total = got_sq[slot_of(0)]
    for k in range(1, n_kv):
        total = total + got_sq[slot_of(k)]
    scale = [lax.rsqrt(t / full_width + out_eps) for t in unpack(total, groups)]
    mixed_ref[...] = projected * jnp.concatenate(scale, axis=0)
    for c in copies_q + copies_kv + copies_att + copies_tp + copies_sq:
        c.wait_send()


def body(
    tokens, norm_gain, w_query, w_key, w_value, head_bias, cache_key, cache_value, lengths, w_out
):
    n_kv, n_tp = lax.axis_size("kv"), lax.axis_size("tp")
    seqs, width_local = tokens.shape
    pos_local, kv_local, head_dim = cache_key.shape[1:]
    heads = head_bias.shape[0]
    out_local = w_out.shape[1]
    chunks = 3 if seqs % 3 == 0 else 1
    assert kv_local == 1 and head_dim == LANES and 2 * heads == SUB and seqs % SUB == 0
    assert heads * (seqs // SUB) <= LANES
    dims = (n_kv, n_tp, seqs, heads, head_dim, pos_local, chunks)
    q_rows = heads * seqs + SUB
    rows = 2 * heads * seqs
    any_spec = pl.BlockSpec(memory_space=pl.ANY)
    smem = pl.BlockSpec(memory_space=pltpu.SMEM)
    vmem = pl.BlockSpec(memory_space=pltpu.VMEM)
    dma = pltpu.SemaphoreType.DMA
    kv_sems = [dma((n_kv - 1,))] * 2
    mixed, new_key, new_value = pl.pallas_call(
        functools.partial(kernel, dims),
        out_shape=(
            jax.ShapeDtypeStruct((seqs, out_local), f32),
            jax.ShapeDtypeStruct((seqs, head_dim), bf16),
            jax.ShapeDtypeStruct((seqs, head_dim), bf16),
        ),
        in_specs=[any_spec] * 5 + [smem] + [any_spec] * 2 + [smem] + [any_spec],
        out_specs=[vmem] * 3,
        scratch_shapes=[
            pltpu.VMEM((seqs, width_local), bf16),
            pltpu.VMEM((1, width_local), f32),
            pltpu.VMEM(w_query.shape, bf16),
            pltpu.VMEM((2,) + w_key.shape, bf16),
            pltpu.VMEM((seqs, pos_local, head_dim), bf16),
            pltpu.VMEM((seqs, pos_local, head_dim), bf16),
            pltpu.VMEM(w_out.shape, bf16),
            pltpu.VMEM((n_kv, q_rows, LANES), f32),
            pltpu.VMEM((n_kv, 2 * seqs, LANES), f32),
            pltpu.VMEM((n_kv, q_rows, LANES), f32),
            pltpu.VMEM((n_tp, seqs, out_local), f32),
            pltpu.VMEM((n_kv, SUB, LANES), f32),
            pltpu.VMEM((rows, head_dim), f32),
            pltpu.VMEM((rows, pos_local), f32),
            pltpu.VMEM((rows, pos_local), f32),
            pltpu.VMEM((rows, head_dim), f32),
            pltpu.VMEM((rows, LANES), f32),
            dma((6,)), dma((chunks,)), dma((chunks,)),
            *kv_sems, *kv_sems, *kv_sems,
            dma((max(n_tp - 1, 1),)), dma((max(n_tp - 1, 1),)),
            *kv_sems,
        ],
        compiler_params=pltpu.CompilerParams(collective_id=0, has_side_effects=True),
    )(
        tokens, norm_gain.reshape(1, width_local), w_query, w_key, w_value, head_bias,
        cache_key.reshape(seqs, pos_local, head_dim), cache_value.reshape(seqs, pos_local, head_dim),
        lengths, w_out,
    )
    return (
        mixed,
        new_key.reshape(seqs, kv_local, head_dim),
        new_value.reshape(seqs, kv_local, head_dim),
    )


def solution(mesh):
    placed = (
        P("dp", "kv"),
        P("kv"),
        P("kv", "tp"),
        P("kv", "tp"),
        P("kv", "tp"),
        P("tp"),
        P("dp", "kv", "tp", None),
        P("dp", "kv", "tp", None),
        P("dp"),
        P("tp", "kv"),
    )
    return jax.shard_map(
        body,
        mesh=mesh,
        in_specs=placed,
        out_specs=(P("dp", "kv"), P("dp", "tp", None), P("dp", "tp", None)),
        check_vma=False,
    )
```

time: 123 us -> 30.1 us (0.24)
  blocking collectives: 67.7 us -> 0 us
  other arithmetic: 28.2 us -> 0 us
  Pallas kernels: 0 us -> 25.2 us
  local copies, waits for them, and re-layouts: 15 us -> 3.99 us
  matrix products: 10.1 us -> 0 us
    psum x3 -> x0, blocking collectives: 40.9 us -> none  [the longest x1 21.6 us: body(): lax.psum((part_query, part_key, part_value), 'kv')]
    all_gather x2 -> x0, blocking collectives: 26.8 us -> none  [the longest x1 13.8 us: body(): lax.all_gather(weighted[None], 'kv', axis=0, tiled=True)]
    pallas_call x0 -> x1, Pallas kernels: none -> 25.2 us  [body(): pl.pallas_call(functools.partial(kernel, dims), out_shape=(jax.ShapeDtype...]
    another operation x3 -> x0, other arithmetic: 22.5 us -> none
    dot_general x6 -> x0, matrix products: 10.1 us -> none  [the longest x1 3.65 us: body(): jnp.einsum('scgp,spcd->scgd', weights, cache_value.astype(jnp.float32), p...]
    another operation x7 -> x0, local copies, waits for them, and re-layouts: 9.53 us -> none
    unnamed x8 -> x3, local copies, waits for them, and re-layouts: 0.49 us -> 3.99 us
    reduce_sum x4 -> x0, other arithmetic: 2.84 us -> none  [the longest x1 1.66 us: body(): decay_total = jnp.sum(penalty, axis=3).reshape(seq_count, heads_local)]
where the time goes in v1:
time: 30.1 us; the launch traced here: 29.8 us
  Pallas kernels  25.2 us (84%)
  local copies, waits for them, and re-layouts  3.99 us (13%)
  between operations  0.64 us (2%)
    pallas_call x1, Pallas kernels, body(): pl.pallas_call(functools.partial(kernel, dims), out_shape=(jax.ShapeDtype...  25.2 us
    unnamed x3, local copies, waits for them, and re-layouts  3.99 us

profile of v1, /device:TPU:0, one launch (start us, length us, event | category | flops | bytes accessed | tf_op | source)
XLA Modules:
  0.0 29.8 jit_solution(10041227375570156818)
XLA Ops:
  0.6 25.2 %shard_map.121 = (f32[24,512]{1,0:T(8,128)}, bf16[24,128]{1,0:T(8,128)(2,1)}, bf16[24,128]{1,0:T(8,128)(2,1)}) custom-call(bf16[24,512]{1,0:T(8,128)(2,1)} %tok_hbm.1, f32[1,512]{1,0:T(1,128)} %bitcast.9, bf16[512,512]{1,0:T(8,128)(2,1)} %wq_hbm.1, bf16[512,128]{1,0:T(8,128)(2,1)} %wk_hbm.1, bf16[512,128]{1,0:T(8,128)(2,1)} %wv_hbm.1, f32[4]{0:T(128)} %bias_ref.1, ...), custom_call_target="tpu_custom_call" | custom-call | tf_op jit(solution)/shard_map/pallas_call | solution.py:232
  25.8 1.4 %copy.16 = f32[24,512]{1,0:T(8,128)} copy(f32[24,512]{1,0:T(8,128)} %get-tuple-element.12) | data formatting | bytes 98304
  27.3 1.3 %copy.17 = bf16[24,1,128]{2,0,1:T(8,128)(2,1)} copy(bf16[24,1,128]{2,0,1:T(8,128)(2,1)} %bitcast.8) | data formatting | bytes 12288
  28.6 1.3 %copy.18 = bf16[24,1,128]{2,0,1:T(8,128)(2,1)} copy(bf16[24,1,128]{2,0,1:T(8,128)(2,1)} %bitcast.7) | data formatting | bytes 12288

commit v2 on v1

v2 whole, which is shorter than its diff:
```python
import functools
import math

import jax
import jax.numpy as jnp
from jax import lax
from jax.experimental import pallas as pl
from jax.experimental.pallas import tpu as pltpu
from jax.sharding import PartitionSpec as P

norm_eps = 1e-06
out_eps = 1e-08
f32 = jnp.float32
bf16 = jnp.bfloat16
SUB = 8
LANES = 128


def kernel(
    dims,
    tok_hbm, gain_hbm, wq_hbm, wk_hbm, wv_hbm, bias_ref, ck_hbm, cv_hbm, len_ref, wo_hbm,
    mixed_ref, nk_ref, nv_ref,
    tok, gain, wq, wkv, ck, cv, wo,
    got_q, got_kv, got_att, got_tp, got_sq, qs, pen_s, ls_s, out_s, tot_s, tri,
    load_sem, key_sem, val_sem,
    send_q, recv_q, send_kv, recv_kv, send_att, recv_att, send_tp, recv_tp, send_sq, recv_sq,
):
    n_kv, n_tp, seqs, heads, head_dim, pos_local, chunks = dims
    me = lax.axis_index("kv")
    me_tp = lax.axis_index("tp")
    groups = seqs // SUB
    width_local = tok.shape[1]
    full_width = width_local * n_kv
    all_pos = pos_local * n_kv

    loads = [
        pltpu.make_async_copy(tok_hbm, tok, load_sem.at[0]),
        pltpu.make_async_copy(gain_hbm, gain, load_sem.at[1]),
        pltpu.make_async_copy(wq_hbm, wq, load_sem.at[2]),
        pltpu.make_async_copy(wk_hbm, wkv.at[0], load_sem.at[3]),
        pltpu.make_async_copy(wv_hbm, wkv.at[1], load_sem.at[4]),
    ]
    for c in loads:
        c.start()
    per = seqs // chunks
    keys = [pltpu.make_async_copy(ck_hbm.at[pl.ds(i * per, per)], ck.at[pl.ds(i * per, per)], key_sem.at[i]) for i in range(chunks)]
    vals = [pltpu.make_async_copy(cv_hbm.at[pl.ds(i * per, per)], cv.at[pl.ds(i * per, per)], val_sem.at[i]) for i in range(chunks)]
    load_wo = pltpu.make_async_copy(wo_hbm, wo, load_sem.at[5])
    for c in keys + vals:
        c.start()
    load_wo.start()

    barrier = pltpu.get_barrier_semaphore()
    for d in range(1, n_kv):
        pl.semaphore_signal(barrier, inc=1, device_id={"kv": lax.rem(me + d, n_kv)}, device_id_type=pl.DeviceIdType.MESH)
    for d in range(1, n_tp):
        pl.semaphore_signal(barrier, inc=1, device_id={"tp": lax.rem(me_tp + d, n_tp)}, device_id_type=pl.DeviceIdType.MESH)

    def spread(buf, rows, send, recv, first, axis, me_axis, n):
        copies = []
        for d in range(1, n):
            at = first * (n - 1) + d - 1
            copies.append(pltpu.make_async_remote_copy(
                src_ref=buf.at[0, rows], dst_ref=buf.at[d, rows], send_sem=send.at[at], recv_sem=recv.at[at],
                device_id={axis: lax.rem(me_axis + d, n)}, device_id_type=pl.DeviceIdType.MESH))
            copies[-1].start()
        return copies

    def slot_of(source):
        return lax.rem(me - source + n_kv, n_kv)

    lane = lax.broadcasted_iota(jnp.int32, (SUB, LANES), 1)

    def pack(columns):
        tile = jnp.zeros((SUB, LANES), f32)
        for c, column in enumerate(columns):
            tile = jnp.where(lane == c, column, tile)
        return tile

    def unpack(tile, count):
        return [jnp.sum(jnp.where(lane == c, tile, 0.0), axis=1, keepdims=True) for c in range(count)]

    loads[0].wait()
    loads[1].wait()
    x = tok[...].astype(f32)
    squares = jnp.sum(x * x, axis=1, keepdims=True)
    scaled = (x * gain[...]).astype(bf16)
    loads[2].wait()
    part_q = jnp.dot(scaled, wq[...], preferred_element_type=f32)
    block = heads * SUB
    got_q[0, :SUB, :] = pack([squares[g * SUB:(g + 1) * SUB] for g in range(groups)])
    for g in range(groups):
        for h in range(heads):
            at = SUB + g * block + h * SUB
            got_q[0, at:at + SUB, :] = part_q[g * SUB:(g + 1) * SUB, h * head_dim:(h + 1) * head_dim]
    pl.semaphore_wait(barrier, n_kv - 1 + n_tp - 1)
    copies_q = []
    for g in range(groups):
        rows = pl.ds(0, SUB + block) if g == 0 else pl.ds(SUB + g * block, block)
        copies_q.append(spread(got_q, rows, send_q, recv_q, g, "kv", me, n_kv))

    later = lax.broadcasted_iota(jnp.int32, (pos_local, pos_local), 0) > lax.broadcasted_iota(jnp.int32, (pos_local, pos_local), 1)
    tri[...] = jnp.where(later, 1.0, 0.0).astype(bf16)
    row = lax.broadcasted_iota(jnp.int32, (2 * heads, 1), 0)
    offset = jnp.zeros((2 * heads, 1), f32)
    for h in range(heads):
        offset = jnp.where(lax.rem(row, heads) == h, bias_ref[h], offset)
    offset = offset - math.log(all_pos)
    high = lax.broadcasted_iota(jnp.int32, (2 * heads, pos_local), 0) < heads
    positions = me * pos_local + lax.broadcasted_iota(jnp.int32, (2 * heads, pos_local), 1)
    loads[3].wait()
    loads[4].wait()
    for i in range(2):
        got_kv[0, i * seqs:(i + 1) * seqs, :] = jnp.dot(scaled, wkv[i], preferred_element_type=f32)

    stride = 2 * heads
    inv = None
    copies_att = []
    for g in range(groups):
        for c in copies_q[g]:
            c.wait_recv()
        rows = slice(0, SUB + block) if g == 0 else slice(SUB + g * block, SUB + (g + 1) * block)
        sum_q = got_q[slot_of(0), rows, :]
        for k in range(1, n_kv):
            sum_q = sum_q + got_q[slot_of(k), rows, :]
        if g == 0:
            inv = [lax.rsqrt(t / full_width + norm_eps) for t in unpack(sum_q[:SUB, :], groups)]
            sum_q = sum_q[SUB:, :]
        base = g * SUB * stride
        for h in range(heads):
            q = (sum_q[h * SUB:(h + 1) * SUB, :] * inv[g]).astype(bf16).astype(f32)
            qs[pl.ds(base + h, SUB, stride=stride), :] = q
            qs[pl.ds(base + heads + h, SUB, stride=stride), :] = q
        keys[g].wait()
        for s in range(g * SUB, (g + 1) * SUB):
            rows = slice(s * stride, (s + 1) * stride)
            score = lax.dot_general(qs[rows, :].astype(bf16), ck[s], (((1,), (1,)), ((), ())), preferred_element_type=f32)
            score = score * head_dim ** (-0.5) + offset
            tail = jnp.log1p(jnp.exp(-jnp.abs(score)))
            visible = positions < len_ref[s]
            penalty = jnp.where(visible, jnp.maximum(score, 0.0) + tail, 0.0)
            top = penalty.astype(bf16).astype(f32)
            pen_s[rows, :] = jnp.where(high, top, penalty - top)
            ls_s[rows, :] = jnp.where(visible, jnp.minimum(score, 0.0) - tail, -1e30)
        suffix = jnp.dot(pen_s[base:base + SUB * stride, :].astype(bf16), tri[...], preferred_element_type=f32)
        vals[g].wait()
        for s in range(g * SUB, (g + 1) * SUB):
            rows = slice(s * stride, (s + 1) * stride)
            between = suffix[s * stride - base:(s + 1) * stride - base, :]
            between = between + pltpu.roll(between, heads, 0)
            weights = jnp.exp(ls_s[rows, :] - between)
            top = weights.astype(bf16).astype(f32)
            parts = jnp.where(high, top, weights - top).astype(bf16)
            out = jnp.dot(parts, cv[s], preferred_element_type=f32)
            out_s[rows, :] = out + pltpu.roll(out, heads, 0)
            first = pen_s[rows, 0:LANES]
            tot_s[rows, :] = between[:, 0:LANES] + first + pltpu.roll(first, heads, 0)
        columns = []
        at = g * (block + SUB)
        for h in range(heads):
            got_att[0, at + h * SUB:at + (h + 1) * SUB, :] = out_s[pl.ds(base + h, SUB, stride=stride), :]
            columns.append(tot_s[pl.ds(base + h, SUB, stride=stride), :][:, 0:1])
        got_att[0, at + block:at + block + SUB, :] = pack(columns)
        copies_att.append(spread(got_att, pl.ds(at, block + SUB), send_att, recv_att, g, "kv", me, n_kv))
    copies_kv = spread(got_kv, pl.ds(0, 2 * seqs), send_kv, recv_kv, 0, "kv", me, n_kv)
    load_wo.wait()

    copies_tp = []
    for g in range(groups):
        for c in copies_att[g]:
            c.wait_recv()
        at = g * (block + SUB)
        pieces = [None] * heads
        behind = jnp.zeros((SUB, LANES), f32)
        for k in reversed(range(n_kv)):
            slot = slot_of(k)
            factor = jnp.exp(-behind)
            behind = behind + got_att[slot, at + block:at + block + SUB, :]
            for h in range(heads):
                term = got_att[slot, at + h * SUB:at + (h + 1) * SUB, :] * factor[:, h:h + 1]
                pieces[h] = term if pieces[h] is None else pieces[h] + term
        attended = jnp.concatenate(pieces, axis=1)
        top = attended.astype(bf16).astype(f32)
        both = jnp.concatenate([top, attended - top], axis=0).astype(bf16)
        partial = jnp.dot(both, wo[...], preferred_element_type=f32)
        got_tp[0, g * SUB:(g + 1) * SUB, :] = partial[:SUB, :] + partial[SUB:, :]
        copies_tp.append(spread(got_tp, pl.ds(g * SUB, SUB), send_tp, recv_tp, g, "tp", me_tp, n_tp))
    projected = []
    columns = []
    for g in range(groups):
        for c in copies_tp[g]:
            c.wait_recv()
        rows = slice(g * SUB, (g + 1) * SUB)
        p = got_tp[lax.rem(me_tp + n_tp, n_tp), rows, :]
        for k in range(1, n_tp):
            p = p + got_tp[lax.rem(me_tp - k + n_tp, n_tp), rows, :]
        projected.append(p)
        columns.append(jnp.sum(p * p, axis=1, keepdims=True))
    got_sq[0] = pack(columns)
    copies_sq = spread(got_sq, pl.ds(0, SUB), send_sq, recv_sq, 0, "kv", me, n_kv)

    for c in copies_kv:
        c.wait_recv()
    sum_kv = got_kv[slot_of(0)]
    for k in range(1, n_kv):
        sum_kv = sum_kv + got_kv[slot_of(k)]
    inv = jnp.concatenate(inv, axis=0)
    nk_ref[...] = (sum_kv[:seqs, :] * inv).astype(bf16)
    nv_ref[...] = (sum_kv[seqs:, :] * inv).astype(bf16)

    for c in copies_sq:
        c.wait_recv()
    total = got_sq[slot_of(0)]
    for k in range(1, n_kv):
        total = total + got_sq[slot_of(k)]
    scale = [lax.rsqrt(t / full_width + out_eps) for t in unpack(total, groups)]
    for g in range(groups):
        mixed_ref[g * SUB:(g + 1) * SUB, :] = projected[g] * scale[g]
    for c in sum(copies_q + copies_att + copies_tp, []) + copies_kv + copies_sq:
        c.wait_send()


def body(
    tokens, norm_gain, w_query, w_key, w_value, head_bias, cache_key, cache_value, lengths, w_out
):
    n_kv, n_tp = lax.axis_size("kv"), lax.axis_size("tp")
    seqs, width_local = tokens.shape
    pos_local, kv_local, head_dim = cache_key.shape[1:]
    heads = head_bias.shape[0]
    out_local = w_out.shape[1]
    chunks = seqs // SUB
    assert kv_local == 1 and head_dim == LANES and 2 * heads == SUB and seqs % SUB == 0
    assert heads * (seqs // SUB) <= LANES
    dims = (n_kv, n_tp, seqs, heads, head_dim, pos_local, chunks)
    q_rows = heads * seqs + SUB
    att_rows = heads * seqs + chunks * SUB
    rows = 2 * heads * seqs
    any_spec = pl.BlockSpec(memory_space=pl.ANY)
    smem = pl.BlockSpec(memory_space=pltpu.SMEM)
    vmem = pl.BlockSpec(memory_space=pltpu.VMEM)
    dma = pltpu.SemaphoreType.DMA
    one = [dma((n_kv - 1,))] * 2
    each = [dma(((n_kv - 1) * chunks,))] * 2
    across = [dma((max(n_tp - 1, 1) * chunks,))] * 2
    mixed, new_key, new_value = pl.pallas_call(
        functools.partial(kernel, dims),
        out_shape=(
            jax.ShapeDtypeStruct((seqs, out_local), f32),
            jax.ShapeDtypeStruct((seqs, head_dim), bf16),
            jax.ShapeDtypeStruct((seqs, head_dim), bf16),
        ),
        in_specs=[any_spec] * 5 + [smem] + [any_spec] * 2 + [smem] + [any_spec],
        out_specs=[vmem] * 3,
        scratch_shapes=[
            pltpu.VMEM((seqs, width_local), bf16),
            pltpu.VMEM((1, width_local), f32),
            pltpu.VMEM(w_query.shape, bf16),
            pltpu.VMEM((2,) + w_key.shape, bf16),
            pltpu.VMEM((seqs, pos_local, head_dim), bf16),
            pltpu.VMEM((seqs, pos_local, head_dim), bf16),
            pltpu.VMEM(w_out.shape, bf16),
            pltpu.VMEM((n_kv, q_rows, LANES), f32),
            pltpu.VMEM((n_kv, 2 * seqs, LANES), f32),
            pltpu.VMEM((n_kv, att_rows, LANES), f32),
            pltpu.VMEM((n_tp, seqs, out_local), f32),
            pltpu.VMEM((n_kv, SUB, LANES), f32),
            pltpu.VMEM((rows, head_dim), f32),
            pltpu.VMEM((rows, pos_local), f32),
            pltpu.VMEM((rows, pos_local), f32),
            pltpu.VMEM((rows, head_dim), f32),
            pltpu.VMEM((rows, LANES), f32),
            pltpu.VMEM((pos_local, pos_local), bf16),
            dma((6,)), dma((chunks,)), dma((chunks,)),
            *each, *one, *each, *across, *one,
        ],
        compiler_params=pltpu.CompilerParams(collective_id=0, has_side_effects=True),
    )(
        tokens, norm_gain.reshape(1, width_local), w_query, w_key, w_value, head_bias,
        cache_key.reshape(seqs, pos_local, head_dim), cache_value.reshape(seqs, pos_local, head_dim),
        lengths, w_out,
    )
    return (
        mixed,
        new_key.reshape(seqs, kv_local, head_dim),
        new_value.reshape(seqs, kv_local, head_dim),
    )


def solution(mesh):
    placed = (
        P("dp", "kv"),
        P("kv"),
        P("kv", "tp"),
        P("kv", "tp"),
        P("kv", "tp"),
        P("tp"),
        P("dp", "kv", "tp", None),
        P("dp", "kv", "tp", None),
        P("dp"),
        P("tp", "kv"),
    )
    return jax.shard_map(
        body,
        mesh=mesh,
        in_specs=placed,
        out_specs=(P("dp", "kv"), P("dp", "tp", None), P("dp", "tp", None)),
        check_vma=False,
    )
```

time: 30.1 us -> 29 us (0.963)
  Pallas kernels: 25.2 us -> 24.1 us
    pallas_call x1, Pallas kernels: 25.2 us -> 24.1 us  [body(): pl.pallas_call(functools.partial(kernel, dims), out_shape=(jax.ShapeDtype...]
where the time goes in v2:
time: 29 us; the launch traced here: 28.7 us
  Pallas kernels  24.1 us (83%)
  local copies, waits for them, and re-layouts  3.99 us (14%)
  between operations  0.64 us (2%)
    pallas_call x1, Pallas kernels, body(): pl.pallas_call(functools.partial(kernel, dims), out_shape=(jax.ShapeDtype...  24.1 us
    unnamed x3, local copies, waits for them, and re-layouts  3.99 us

profile of v2, /device:TPU:0, one launch (start us, length us, event | category | flops | bytes accessed | tf_op | source)
XLA Modules:
  0.0 28.7 jit_solution(5435864080991010487)
XLA Ops:
  0.6 24.1 %shard_map.121 = (f32[24,512]{1,0:T(8,128)}, bf16[24,128]{1,0:T(8,128)(2,1)}, bf16[24,128]{1,0:T(8,128)(2,1)}) custom-call(bf16[24,512]{1,0:T(8,128)(2,1)} %tok_hbm.1, f32[1,512]{1,0:T(1,128)} %bitcast.9, bf16[512,512]{1,0:T(8,128)(2,1)} %wq_hbm.1, bf16[512,128]{1,0:T(8,128)(2,1)} %wk_hbm.1, bf16[512,128]{1,0:T(8,128)(2,1)} %wv_hbm.1, f32[4]{0:T(128)} %bias_ref.1, ...), custom_call_target="tpu_custom_call" | custom-call | tf_op jit(solution)/shard_map/pallas_call | solution.py:245
  24.7 1.4 %copy.16 = f32[24,512]{1,0:T(8,128)} copy(f32[24,512]{1,0:T(8,128)} %get-tuple-element.12) | data formatting | bytes 98304
  26.2 1.3 %copy.17 = bf16[24,1,128]{2,0,1:T(8,128)(2,1)} copy(bf16[24,1,128]{2,0,1:T(8,128)(2,1)} %bitcast.8) | data formatting | bytes 12288
  27.4 1.3 %copy.18 = bf16[24,1,128]{2,0,1:T(8,128)(2,1)} copy(bf16[24,1,128]{2,0,1:T(8,128)(2,1)} %bitcast.7) | data formatting | bytes 12288
